TPU v7x, 32 devices: a whole 2x2x4 slice. The times are simulated.
32 devices in a mesh: ep: 16 (over z, y, x), tp: 2 (over core).
Axes of the slice: x: 2, y: 2, z: 4, core: 2. Of those that a mesh axis runs over, the one named last changes fastest.
Arguments:
- tokens_in: bfloat16 [512, 2048], P('ep'), may hold values from -6 to 6
- state_in: float32 [512, 8, 64, 64], P('ep', 'tp'), may hold values from -4 to 4
- norm_mix: bfloat16 [2048], replicated, may hold values from 0.099609375 to 1.8984375
- w_recept: bfloat16 [2048, 512], P(None, 'tp'), may hold values from -0.125 to 0.125
- w_key: bfloat16 [2048, 512], P(None, 'tp'), may hold values from -0.125 to 0.125
- w_value: bfloat16 [2048, 512], P(None, 'tp'), may hold values from -0.125 to 0.125
- decay_down: bfloat16 [2048, 64], replicated, may hold values from -0.125 to 0.125
- decay_up: bfloat16 [64, 512], P(None, 'tp'), may hold values from -0.75 to 0.75
- decay_base: float32 [512], P('tp'), may hold values from -4 to 2
- iclr_down: bfloat16 [2048, 64], replicated, may hold values from -0.125 to 0.125
- iclr_up: bfloat16 [64, 512], P(None, 'tp'), may hold values from -0.75 to 0.75
- iclr_base: float32 [512], P('tp'), may hold values from -4 to 4
- key_scale: bfloat16 [512], P('tp'), may hold values from 0.099609375 to 1.8984375
- key_mix: bfloat16 [512], P('tp'), may hold values from 0.099609375 to 1.8984375
- w_out: bfloat16 [512, 2048], P('tp'), may hold values from -0.046875 to 0.046875
- norm_moe: bfloat16 [2048], replicated, may hold values from 0.099609375 to 1.8984375
- router_group: bfloat16 [2048, 2], replicated, may hold values from -0.125 to 0.125
- router_expert: bfloat16 [2048, 16], replicated, may hold values from -0.125 to 0.125
- routes: int32 [512, 4], P('ep'), may hold values from 0 to 15, as said below
- expert_gate: bfloat16 [16, 2048, 256], P('ep', None, 'tp'), may hold values from -0.125 to 0.125
- expert_up: bfloat16 [16, 2048, 256], P('ep', None, 'tp'), may hold values from -0.125 to 0.125
- expert_down: bfloat16 [16, 256, 2048], P('ep', 'tp'), may hold values from -1.5 to 1.5
Outputs:
- layer_out: bfloat16 [512, 2048], P('ep', 'tp')
- state_out: float32 [512, 8, 64, 64], P('ep', 'tp')
Inputs may be any that keep to these rules, and one draw needn't show every extreme that they name: `routes`: each row names 4 different experts of one group (the same value of id // 8). Among the rows of one device no expert is named by more than 16 rows, and in every draw one expert is named by exactly 16 rows of every device.
All inputs are finite; a program needn't handle non-finite values.
Results may differ from a plain program's by a relative error of at most 0.018.
Values may be sent and summed in bfloat16 or wider, within the bound.
A program may use at most 64 MiB of HBM per device.

v0:
```python
import jax
import jax.numpy as jnp
from jax import lax
from jax.sharding import PartitionSpec as P


def rms_scale(values, weights):
    values32 = values.astype(jnp.float32)
    factor = lax.rsqrt(jnp.mean(values32 * values32, axis=-1, keepdims=True) + 1e-06)
    return (values32 * factor * weights.astype(jnp.float32)).astype(jnp.bfloat16)


def shards(
    tokens_in,
    state_in,
    norm_mix,
    w_recept,
    w_key,
    w_value,
    decay_down,
    decay_up,
    decay_base,
    iclr_down,
    iclr_up,
    iclr_base,
    key_scale,
    key_mix,
    w_out,
    norm_moe,
    router_group,
    router_expert,
    routes,
    expert_gate,
    expert_up,
    expert_down,
):
    f32 = jnp.float32
    bf16 = jnp.bfloat16
    seq_count = tokens_in.shape[0]
    width_model = tokens_in.shape[1]
    heads_here = state_in.shape[1]
    head_size = state_in.shape[-1]
    tp_count = lax.axis_size("tp")
    ep_count = lax.axis_size("ep")
    half_width = width_model // tp_count

    def split_heads(values):
        return values.astype(f32).reshape(values.shape[0], heads_here, head_size)

    normed = rms_scale(tokens_in, norm_mix)
    recept = jnp.dot(normed, w_recept, preferred_element_type=f32).astype(bf16)
    key_rows = jnp.dot(normed, w_key, preferred_element_type=f32).astype(bf16)
    value_rows = jnp.dot(normed, w_value, preferred_element_type=f32).astype(bf16)
    decay_low = jnp.tanh(jnp.dot(normed, decay_down, preferred_element_type=f32)).astype(bf16)
    iclr_low = jnp.dot(normed, iclr_down, preferred_element_type=f32).astype(bf16)
    log_rate = (
        -jax.nn.softplus(-(decay_base + jnp.dot(decay_low, decay_up, preferred_element_type=f32)))
        - 0.5
    )
    decays = jnp.exp(-jnp.exp(log_rate))
    learn_rate = jax.nn.sigmoid(iclr_base + jnp.dot(iclr_low, iclr_up, preferred_element_type=f32))
    recept_heads = split_heads(recept)
    key_heads = split_heads(key_rows)
    value_heads = split_heads(value_rows)
    rate_heads = split_heads(learn_rate)
    decay_heads = split_heads(decays)
    scaled = key_heads * key_scale.astype(f32).reshape(heads_here, head_size)
    unit_key = scaled * lax.rsqrt(jnp.sum(scaled * scaled, axis=-1, keepdims=True) + 1e-06)
    key_mod = key_heads * (
        1.0 + (rate_heads - 1.0) * key_mix.astype(f32).reshape(heads_here, head_size)
    )
    removed = jnp.einsum("shvk,shk->shv", state_in, unit_key)
    state_out = (
        state_in * decay_heads[:, :, None, :]
        - removed[..., None] * (unit_key * rate_heads)[:, :, None, :]
        + value_heads[..., None] * key_mod[:, :, None, :]
    )
    mixed = (
        jnp.einsum("shvk,shk->shv", state_out, recept_heads)
        .reshape(seq_count, heads_here * head_size)
        .astype(bf16)
    )
    partial_value = jnp.dot(mixed, w_out, preferred_element_type=f32)
    mixer_out = lax.psum(partial_value, "tp").astype(bf16)
    x_mid = (tokens_in.astype(f32) + mixer_out.astype(f32)).astype(bf16)
    own_half = lax.dynamic_slice_in_dim(x_mid, lax.axis_index("tp") * half_width, half_width, 1)
    moe_in = rms_scale(x_mid, norm_moe)
    n_groups = router_group.shape[1]
    experts_all = router_expert.shape[1]
    group_size = experts_all // n_groups
    top_count = routes.shape[1]
    group_id = routes[:, 0] // group_size
    group_logit = jnp.dot(moe_in, router_group, preferred_element_type=f32)
    group_hit = group_id[:, None] == jnp.arange(n_groups)[None, :]
    group_prob = jax.nn.sigmoid(jnp.sum(jnp.where(group_hit, group_logit, 0.0), axis=1))
    expert_logit = jnp.dot(moe_in, router_expert, preferred_element_type=f32)
    expert_hit = routes[:, :, None] == jnp.arange(experts_all)[None, None, :]
    scores = jax.nn.sigmoid(jnp.sum(jnp.where(expert_hit, expert_logit[:, None, :], 0.0), axis=2))
    route_weight = group_prob[:, None] * scores / jnp.sum(scores, axis=1, keepdims=True)
    capacity = max(2, 2 * seq_count * top_count // ep_count)
    flat_routes = routes.reshape(-1)
    slot_count = flat_routes.shape[0]
    matches = flat_routes[:, None] == flat_routes[None, :]
    earlier = jnp.arange(slot_count)[:, None] < jnp.arange(slot_count)[None, :]
    position = jnp.sum(jnp.logical_and(matches, earlier).astype(jnp.int32), axis=0)
    target = flat_routes * capacity + position
    buffer_rows = experts_all * capacity
    placement = jnp.sum(
        (
            target.reshape(seq_count, top_count)[:, :, None]
            == jnp.arange(buffer_rows)[None, None, :]
        ).astype(bf16),
        axis=1,
    )
    outgoing = jnp.einsum("se,sd->ed", placement, moe_in, preferred_element_type=f32).astype(bf16)
    outgoing = outgoing.reshape(experts_all, capacity, moe_in.shape[1])
    incoming = lax.all_to_all(outgoing, "ep", split_axis=0, concat_axis=0, tiled=True)
    flat_rows = incoming.reshape(-1, width_model)
    gate_part = jnp.dot(flat_rows, expert_gate[0], preferred_element_type=f32)
    up_part = jnp.dot(flat_rows, expert_up[0], preferred_element_type=f32)
    hidden = (jax.nn.silu(gate_part) * up_part).astype(bf16)
    partial_out = jnp.dot(hidden, expert_down[0], preferred_element_type=f32)
    partial_out = partial_out.reshape(incoming.shape[0], incoming.shape[1], width_model)
    result = (
        lax.psum_scatter(partial_out.astype(jnp.bfloat16), "tp", scatter_dimension=2, tiled=True)
        .astype(jnp.float32)
        .astype(bf16)
    )
    returned = lax.all_to_all(result, "ep", split_axis=0, concat_axis=0, tiled=True)
    flat_back = returned.reshape(buffer_rows, half_width)
    chooser = (target[:, None] == jnp.arange(buffer_rows)[None, :]).astype(bf16)
    gathered = jnp.dot(chooser, flat_back, preferred_element_type=f32).reshape(
        seq_count, top_count, half_width
    )
    moe_out = jnp.sum(route_weight[:, :, None] * gathered, axis=1)
    layer_out = (own_half.astype(f32) + moe_out).astype(bf16)
    return (layer_out, state_out)


def solution(mesh):
    in_specs = (
        P("ep", None),
        P("ep", "tp", None, None),
        P(),
        P(None, "tp"),
        P(None, "tp"),
        P(None, "tp"),
        P(),
        P(None, "tp"),
        P("tp"),
        P(),
        P(None, "tp"),
        P("tp"),
        P("tp"),
        P("tp"),
        P("tp", None),
        P(),
        P(),
        P(),
        P("ep", None),
        P("ep", None, "tp"),
        P("ep", None, "tp"),
        P("ep", "tp", None),
    )
    out_specs = (P("ep", "tp"), P("ep", "tp", None, None))
    return jax.shard_map(shards, mesh=mesh, in_specs=in_specs, out_specs=out_specs, check_vma=False)
```

profile of v0, /device:TPU:0, one launch (start us, length us, event | category | flops | bytes accessed | tf_op | source)
XLA Modules:
  0.0 107.7 jit_solution(8539937595506873282)
XLA Ops:
  7.2 0.8 convert_element_type.81
  8.1 1.0 fusion.18
  9.1 1.6 %fusion.8 = f32[32,256]{1,0:T(8,128)S(1)} fusion(bf16[2048,256]{1,0:T(8,128)(2,1)} %param.26, bf16[32,2048]{1,0:T(8,128)(2,1)} %param.22, f32[2048]{0:T(1024)S(1)} %convert_element_type.81, f32[32]{0:T(128)S(1)} %add_rsqrt_fusion.2), kind=kOutput, calls=%fused_computation.18 | convolution fusion | flops 33832960 | bytes 1220736 | tf_op jit(solution)/shard_map/dot_general | solution.py:52
  10.9 0.7 reshape.178
  11.6 0.1 multiply_reduce_fusion
  11.7 1.4 %fusion.5 = f32[32,256]{1,0:T(8,128)S(1)} fusion(bf16[64,256]{1,0:T(8,128)(2,1)} %param.32, bf16[2048,64]{0,1:T(8,128)(2,1)} %param.31, f32[256]{0:T(256)} %param.33, bf16[32,2048]{1,0:T(8,128)(2,1)} %param.22, f32[2048]{0:T(1024)S(1)} %convert_element_type.81, f32[32]{0:T(128)S(1)} %add_rsqrt_fusion.2), kind=kOutput, calls=%fused_computation.11 | convolution fusion | flops 9734144 | bytes 468096 | tf_op jit(solution)/shard_map/dot_general | solution.py:61
  13.2 0.7 reshape.180
  14.0 1.4 %fusion.32 = f32[32,256]{1,0:T(8,128)S(1)} fusion(bf16[64,256]{1,0:T(8,128)(2,1)} %param.29, bf16[2048,64]{0,1:T(8,128)(2,1)} %param.28, f32[256]{0:T(256)} %param.30, bf16[32,2048]{1,0:T(8,128)(2,1)} %param.22, f32[2048]{0:T(1024)S(1)} %convert_element_type.81, f32[32]{0:T(128)S(1)} %add_rsqrt_fusion.2), kind=kOutput, calls=%fused_computation.58 | convolution fusion | flops 9791488 | bytes 468096 | tf_op jit(solution)/shard_map/dot_general | solution.py:57
  15.5 1.6 %fusion.7 = f32[32,256]{1,0:T(8,128)S(1)} fusion(bf16[2048,256]{1,0:T(8,128)(2,1)} %param.27, bf16[32,2048]{1,0:T(8,128)(2,1)} %param.22, f32[2048]{0:T(1024)S(1)} %convert_element_type.81, f32[32]{0:T(128)S(1)} %add_rsqrt_fusion.2), kind=kOutput, calls=%fused_computation.16 | convolution fusion | flops 33832960 | bytes 1220736 | tf_op jit(solution)/shard_map/dot_general | solution.py:53
  17.2 0.3 convolution_convert_fusion.2
  17.7 0.1 fusion.47
  17.8 3.5 %fusion.48 = f32[32,4,1,64]{3,2,1,0:T(1,128)S(1)} fusion(f32[32,4,64,1]{2,3,1,0:T(1,128)S(1)} %bitcast.54, f32[32,4,64,64]{3,2,1,0:T(8,128)} %param.23), kind=kOutput, calls=%fused_computation.76 | convolution fusion | flops 1048576 | bytes 2162688 | tf_op jit(solution)/shard_map/shvk,shk->shv/dot_general | solution.py:72
  21.3 2.7 %multiply_add_fusion = f32[32,4,64,64]{3,2,1,0:T(8,128)S(1)} fusion(f32[32,4,64,64]{3,2,1,0:T(8,128)S(1)} %copy-done.1, f32[32,4,64]{2,1,0:T(4,128)S(1)} %get-tuple-element.6, f32[32,4,64]{2,1,0:T(4,128)S(1)} %reshape.179, f32[32,4,64]{2,1,0:T(4,128)S(1)} %get-tuple-element.4, f32[32,4,64]{2,1,0:T(4,128)S(1)} %bitcast.52, f32[32,4,64]{2,1,0:T(4,128)S(1)} %mul.189), kind=kLoop, calls=%fused_computation | loop fusion | flops 2621440 | bytes 4358144 | tf_op jit(solution)/shard_map/add | solution.py:74
  24.1 2.0 %copy-done.2 = f32[32,4,64,64]{3,2,1,0:T(8,128)} copy-done((f32[32,4,64,64]{3,2,1,0:T(8,128)}, f32[32,4,64,64]{3,2,1,0:T(8,128)S(1)}, u32[]{:S(2)}) %copy-start.2) | copy-done | bytes 2097176
  26.1 1.2 %fusion.49 = f32[32,4,1,64]{3,2,1,0:T(1,128)S(1)} fusion(f32[32,4,64,64]{3,2,1,0:T(8,128)S(1)} %multiply_add_fusion, bf16[32,4,64,1]{2,3,1,0:T(2,128)(2,1)S(1)} %reshape.188), kind=kOutput, calls=%fused_computation.77 | convolution fusion | flops 1048576 | bytes 2146304 | tf_op jit(solution)/shard_map/shvk,shk->shv/dot_general | solution.py:79
  27.4 0.3 fusion.50
  27.7 4.6 %all-reduce.1 = bf16[32,2048]{1,0:T(8,128)(2,1)S(1)} all-reduce(f32[32,2048]{1,0:T(8,128)S(1)} %fusion.50), channel_id=1, replica_groups=mesh['ep'=16,'tp'=2] {'tp'}, use_global_device_ids=true, to_apply=%region_2.3 | all-reduce | flops 65536 | bytes 393216 | tf_op jit(solution)/shard_map/psum | solution.py:84
  32.3 0.2 fusion.15
  32.6 0.1 eq.92
  32.7 0.1 convert_reduce_fusion
  33.1 0.5 convolution_convert_fusion.1
  33.6 34.7 %all_to_all.10 = bf16[16,16,2048]{2,1,0:T(8,128)(2,1)S(1)} all-to-all(bf16[16,16,2048]{2,1,0:T(8,128)(2,1)S(1)} %bitcast.48), channel_id=1, replica_groups=mesh['ep'=16,'tp'=2] {'ep'}, dimensions={0} | all-to-all | bytes 2097152 | tf_op jit(solution)/shard_map/all_to_all | solution.py:117
  68.3 0.4 fusion.13
  68.7 0.4 fusion.1
  69.2 1.4 %convolution_convert_fusion = bf16[16,16,2048]{2,1,0:T(8,128)(2,1)} fusion(bf16[16,16,128]{2,1,0:T(8,128)(2,1)S(1)} %bitcast.55, bf16[1,128,2048]{2,1,0:T(8,128)(2,1)S(1)} %copy-done.5), kind=kOutput, calls=%fused_computation.1 | convolution fusion | flops 134742016 | bytes 1638400 | tf_op jit(solution)/shard_map/dot_general | solution.py:122
  70.6 0.2 fusion.36
  70.9 6.8 %reduce-scatter.2.cloned.1.call-done = bf16[16,16,1024]{2,1,0:T(8,128)(2,1)} async-done(((bf16[16,16,2048]{2,1,0:T(8,128)(2,1)}), bf16[16,16,1024]{2,1,0:T(8,128)(2,1)}) %reduce-scatter.2.cloned.1.call-update) | async-done | bytes 524304 | tf_op jit(solution)/shard_map/reduce_scatter | solution.py:125
  77.6 6.8 %all-to-all-start.1 = ((bf16[16,16,1024]{2,1,0:T(8,128)(2,1)}), bf16[16,16,1024]{2,1,0:T(8,128)(2,1)S(1)}, u32[]{:S(2)}, u32[]{:S(2)}) async-start(bf16[16,16,1024]{2,1,0:T(8,128)(2,1)} %reduce-scatter.2.cloned.1.call-done), calls=%async_computation.2 | async-start | bytes 1048576 | tf_op jit(solution)/shard_map/all_to_all | solution.py:129
  84.5 0.2 fusion.10
  84.7 15.1 %all-to-all-done.1 = bf16[16,16,1024]{2,1,0:T(8,128)(2,1)S(1)} async-done(((bf16[16,16,1024]{2,1,0:T(8,128)(2,1)}), bf16[16,16,1024]{2,1,0:T(8,128)(2,1)S(1)}, u32[]{:S(2)}, u32[]{:S(2)}) %all-to-all-start.1) | async-done | bytes 524320 | tf_op jit(solution)/shard_map/all_to_all | solution.py:129
  99.9 0.3 fusion
  100.2 0.7 add_convert_fusion
  (46 shorter events, 1.2 us)
Async XLA Ops:
  7.2 20.2 %copy-start = (bf16[256,2048]{1,0:T(8,128)(2,1)S(1)}, bf16[256,2048]{1,0:T(8,128)(2,1)}, u32[]{:S(2)}) copy-start(bf16[256,2048]{1,0:T(8,128)(2,1)} %param.36) | copy-start | bytes 3145732
  7.2 10.0 %copy-start.3 = (bf16[32,2048]{1,0:T(8,128)(2,1)S(1)}, bf16[32,2048]{1,0:T(8,128)(2,1)}, u32[]{:S(2)}) copy-start(bf16[32,2048]{1,0:T(8,128)(2,1)} %param.22) | copy-start | bytes 393220
  7.2 10.0 %copy-start.4 = (bf16[2048,256]{1,0:T(8,128)(2,1)S(1)}, bf16[2048,256]{1,0:T(8,128)(2,1)}, u32[]{:S(2)}) copy-start(bf16[2048,256]{1,0:T(8,128)(2,1)} %param.25) | copy-start | bytes 3145732
  7.2 70.4 %reduce-scatter.2.cloned.1.call-start = ((), (), s32[]{:S(2)}) async-start(), calls=%async_computation.3 | async-start | bytes 1572864 | tf_op jit(solution)/shard_map/reduce_scatter | solution.py:125
  17.7 3.6 %copy-start.1 = (f32[32,4,64,64]{3,2,1,0:T(8,128)S(1)}, f32[32,4,64,64]{3,2,1,0:T(8,128)}, u32[]{:S(2)}) copy-start(f32[32,4,64,64]{3,2,1,0:T(8,128)} %param.23) | copy-start | bytes 6291460
  24.1 2.0 %copy-start.2 = (f32[32,4,64,64]{3,2,1,0:T(8,128)}, f32[32,4,64,64]{3,2,1,0:T(8,128)S(1)}, u32[]{:S(2)}) copy-start(f32[32,4,64,64]{3,2,1,0:T(8,128)S(1)} %multiply_add_fusion) | copy-start | bytes 6291460
  26.1 6.4 %copy-start.8 = (bf16[2048]{0:T(1024)(128)(2,1)S(1)}, bf16[2048]{0:T(1024)(128)(2,1)}, u32[]{:S(2)}) copy-start(bf16[2048]{0:T(1024)(128)(2,1)} %param.37) | copy-start | bytes 12292
  26.1 6.4 %copy-start.7 = (s32[32,4]{0,1:T(4,128)S(1)}, s32[32,4]{0,1:T(4,128)}, u32[]{:S(2)}) copy-start(s32[32,4]{0,1:T(4,128)} %param.40) | copy-start | bytes 1540
  26.1 42.2 %copy-start.6 = (bf16[1,2048,128]{2,1,0:T(8,128)(2,1)S(1)}, bf16[1,2048,128]{2,1,0:T(8,128)(2,1)}, u32[]{:S(2)}) copy-start(bf16[1,2048,128]{2,1,0:T(8,128)(2,1)} %param.41) | copy-start | bytes 1572868
  27.3 41.5 %copy-start.9 = (bf16[1,2048,128]{2,1,0:T(8,128)(2,1)S(1)}, bf16[1,2048,128]{2,1,0:T(8,128)(2,1)}, u32[]{:S(2)}) copy-start(bf16[1,2048,128]{2,1,0:T(8,128)(2,1)} %param.42) | copy-start | bytes 1572868
  27.7 41.5 %copy-start.5 = (bf16[1,128,2048]{2,1,0:T(8,128)(2,1)S(1)}, bf16[1,128,2048]{2,1,0:T(8,128)(2,1)}, u32[]{:S(2)}) copy-start(bf16[1,128,2048]{2,1,0:T(8,128)(2,1)} %param.43) | copy-start | bytes 1572868
  33.6 37.0 %copy-start.10 = (bf16[2048,16]{0,1:T(8,128)(2,1)S(1)}, bf16[2048,16]{0,1:T(8,128)(2,1)}, u32[]{:S(2)}) copy-start(bf16[2048,16]{0,1:T(8,128)(2,1)} %param.39) | copy-start | bytes 196612
  68.3 16.2 %copy-start.11 = (bf16[2048,2]{0,1:T(2,128)(2,1)S(1)}, bf16[2048,2]{0,1:T(2,128)(2,1)}, u32[]{:S(2)}) copy-start(bf16[2048,2]{0,1:T(2,128)(2,1)} %param.38) | copy-start | bytes 24580
  77.6 22.3 %all-to-all-start.1 = ((bf16[16,16,1024]{2,1,0:T(8,128)(2,1)}), bf16[16,16,1024]{2,1,0:T(8,128)(2,1)S(1)}, u32[]{:S(2)}, u32[]{:S(2)}) async-start(bf16[16,16,1024]{2,1,0:T(8,128)(2,1)} %reduce-scatter.2.cloned.1.call-done), calls=%async_computation.2 | async-start | bytes 1048576 | tf_op jit(solution)/shard_map/all_to_all | solution.py:129
Sparse Core Ops, SparseCore 0:
  70.8 6.8 reduce-scatter.1
where the time goes:
time: 108 us
  blocking collectives  39.3 us (36%)
  waiting for transfers between devices  21.9 us (20%)
  matrix products  14.8 us (14%)
  between operations  14.3 us (13%)
  starting transfers between devices  6.81 us (6%)
  other arithmetic  6 us (6%)
  local copies, waits for them, and re-layouts  4.48 us (4%)
    all_to_all x1, blocking collectives, shards(): lax.all_to_all(outgoing, 'ep', split_axis=0, concat_axis=0, tiled=True)  34.7 us
    all_to_all x1, waiting for transfers between devices, shards(): lax.all_to_all(result, 'ep', split_axis=0, concat_axis=0, tiled=True)  15.1 us
    all_to_all x1, starting transfers between devices, shards(): lax.all_to_all(result, 'ep', split_axis=0, concat_axis=0, tiled=True)  6.77 us
    reduce_scatter x1, waiting for transfers between devices, shards(): lax.psum_scatter(partial_out.astype(jnp.bfloat16), 'tp', scatter_dimensio...  6.75 us
    psum x1, blocking collectives, shards(): mixer_out = lax.psum(partial_value, 'tp').astype(bf16)  4.64 us
    dot_general x1, matrix products, shards(): removed = jnp.einsum('shvk,shk->shv', state_in, unit_key)  3.51 us
    add x1, other arithmetic, shards(): state_in * decay_heads[:, :, None, :]  2.75 us
  transfers between devices with their start and end apart: 2, of which 2 were waited for; matrix products, arithmetic and copies ran while one was open for 0% of the time, Pallas kernels for 0%

commit v1 on v0

v1 whole, which is shorter than its diff:
```python
import functools

import jax
import jax.numpy as jnp
from jax import lax
from jax.experimental import pallas as pl
from jax.experimental.pallas import tpu as pltpu
from jax.sharding import PartitionSpec as P


def rms_scale(values, weights):
    values32 = values.astype(jnp.float32)
    factor = lax.rsqrt(jnp.mean(values32 * values32, axis=-1, keepdims=True) + 1e-06)
    return (values32 * factor * weights.astype(jnp.float32)).astype(jnp.bfloat16)


def moe_kernel(
    ep_count,
    block_rows,
    mixed_ref,
    w_out_ref,
    tokens_ref,
    norm_ref,
    router_group_ref,
    router_expert_ref,
    group_hit_ref,
    uses_ref,
    placement_ref,
    chooser_ref,
    gate_ref,
    up_ref,
    down_ref,
    out_ref,
    part_buf,
    part_recv,
    mid_buf,
    norm_buf,
    send_buf,
    rows_buf,
    hidden_buf,
    term_send,
    term_own,
    term_recv,
    result_buf,
    back_buf,
    part_sems,
    out_send_sems,
    out_recv_sems,
    pair_send_sems,
    pair_recv_sems,
    term_send_sems,
    term_recv_sems,
    back_send_sems,
    back_recv_sems,
):
    f32 = jnp.float32
    bf16 = jnp.bfloat16
    me = lax.axis_index("ep")
    core = lax.axis_index("tp")
    other = 1 - core
    seq_count, width = tokens_ref.shape
    half = width // 2
    cap = send_buf.shape[1]
    total_rows = ep_count * cap
    per_block = block_rows // cap
    n_blocks = total_rows // block_rows
    mesh_ids = pl.DeviceIdType.MESH

    def peer_at(step):
        return lax.rem(me + step, ep_count)

    def step_at(index):
        return 1 + lax.rem(index + ep_count // 2 - 1, ep_count - 1)

    barrier = pltpu.get_barrier_semaphore()
    pl.semaphore_signal(barrier, inc=1, device_id=(me, other), device_id_type=mesh_ids)

    def greet(step, carry):
        pl.semaphore_signal(
            barrier, inc=1, device_id=(peer_at(step), core), device_id_type=mesh_ids
        )
        return carry

    lax.fori_loop(1, ep_count, greet, 0)

    for index in range(2):
        columns = slice(index * half, (index + 1) * half)
        part_buf[index] = jnp.dot(
            mixed_ref[...], w_out_ref[:, columns], preferred_element_type=f32
        )
    pl.semaphore_wait(barrier, ep_count)

    def pair_copy(source, target, send_sem, recv_sem):
        return pltpu.make_async_remote_copy(
            src_ref=source,
            dst_ref=target,
            send_sem=send_sem,
            recv_sem=recv_sem,
            device_id=(me, other),
            device_id_type=mesh_ids,
        )

    part_copy = pair_copy(part_buf, part_recv, part_sems.at[0], part_sems.at[1])
    part_copy.start()
    part_copy.wait()

    squares = jnp.zeros((seq_count, 1), f32)
    for index in range(2):
        columns = slice(index * half, (index + 1) * half)
        mixer_out = (part_buf[index] + part_recv[index]).astype(bf16)
        mid = (tokens_ref[:, columns].astype(f32) + mixer_out.astype(f32)).astype(bf16)
        mid_buf[index] = mid
        mid32 = mid.astype(f32)
        squares = squares + jnp.sum(mid32 * mid32, axis=1, keepdims=True)
    factor = lax.rsqrt(squares / width + 1e-06)
    for index in range(2):
        columns = slice(index * half, (index + 1) * half)
        norm_buf[index] = (
            mid_buf[index].astype(f32) * factor * norm_ref[:, columns].astype(f32)
        ).astype(bf16)

    own_norm = norm_buf[core]
    for index in range(n_blocks):
        rows = jnp.dot(
            placement_ref[index * block_rows : (index + 1) * block_rows, :],
            own_norm,
            preferred_element_type=f32,
        ).astype(bf16)
        send_buf[index * per_block : (index + 1) * per_block] = rows.reshape(per_block, cap, half)

    def out_copy(step):
        peer = peer_at(step)
        return pltpu.make_async_remote_copy(
            src_ref=send_buf.at[peer],
            dst_ref=rows_buf.at[core, me],
            send_sem=out_send_sems.at[step],
            recv_sem=out_recv_sems.at[step],
            device_id=(peer, core),
            device_id_type=mesh_ids,
        )

    def rows_copy(step):
        source = lax.rem(me + ep_count - step, ep_count)
        return pair_copy(
            rows_buf.at[core, source],
            rows_buf.at[core, source],
            pair_send_sems.at[step],
            pair_recv_sems.at[step],
        )

    def rows_arrival(step):
        source = lax.rem(me + ep_count - step, ep_count)
        return pair_copy(
            rows_buf.at[other, source],
            rows_buf.at[other, source],
            pair_send_sems.at[step],
            pair_recv_sems.at[step],
        )

    def start_out(index, carry):
        out_copy(step_at(index)).start()
        return carry

    lax.fori_loop(0, ep_count - 1, start_out, 0)
    rows_buf[core, me] = send_buf[me]
    rows_copy(0).start()

    group_logit = jnp.zeros(group_hit_ref.shape, f32)
    expert_logit = jnp.zeros(uses_ref.shape, f32)
    for index in range(2):
        columns = slice(index * half, (index + 1) * half)
        group_logit += jnp.dot(
            norm_buf[index], router_group_ref[columns, :], preferred_element_type=f32
        )
        expert_logit += jnp.dot(
            norm_buf[index], router_expert_ref[columns, :], preferred_element_type=f32
        )
    group_prob = jax.nn.sigmoid(jnp.sum(group_logit * group_hit_ref[...], axis=1, keepdims=True))
    scores = jax.nn.sigmoid(expert_logit) * uses_ref[...]
    weights = group_prob * scores / jnp.sum(scores, axis=1, keepdims=True)
    weights_high = weights.astype(bf16)
    weights_low = (weights - weights_high.astype(f32)).astype(bf16)
    slot_expert = lax.broadcasted_iota(jnp.int32, (ep_count, total_rows), 1) // cap
    expert_ids = lax.broadcasted_iota(jnp.int32, (ep_count, total_rows), 0)
    spread = jnp.where(slot_expert == expert_ids, 1.0, 0.0).astype(bf16)
    chooser = chooser_ref[...].astype(f32)
    combine_high = (jnp.dot(weights_high, spread, preferred_element_type=f32) * chooser).astype(bf16)
    combine_low = (jnp.dot(weights_low, spread, preferred_element_type=f32) * chooser).astype(bf16)

    def relay(index, carry):
        step = step_at(ep_count - 2 - index)
        out_copy(step).wait_recv()
        rows_copy(step).start()
        return carry

    lax.fori_loop(0, ep_count - 1, relay, 0)

    def arrive(step, carry):
        rows_arrival(step).wait_recv()
        return carry

    lax.fori_loop(0, ep_count, arrive, 0)

    for index in range(n_blocks):
        experts = slice(index * per_block, (index + 1) * per_block)
        gate_part = jnp.zeros((block_rows, gate_ref.shape[1]), f32)
        up_part = jnp.zeros((block_rows, gate_ref.shape[1]), f32)
        for piece in range(2):
            columns = slice(piece * half, (piece + 1) * half)
            rows = rows_buf[piece, experts].reshape(block_rows, half)
            gate_part += jnp.dot(rows, gate_ref[columns, :], preferred_element_type=f32)
            up_part += jnp.dot(rows, up_ref[columns, :], preferred_element_type=f32)
        hidden = (gate_part / (1.0 + jnp.exp(-gate_part)) * up_part).astype(bf16)
        hidden_buf[experts] = hidden.reshape(per_block, cap, gate_ref.shape[1])

    n_parts = term_send.shape[0]
    per_part = ep_count // n_parts
    first_part = me // per_part

    def part_at(index):
        return lax.rem(first_part + index + n_parts // 2, n_parts)

    def term_copy(part):
        return pair_copy(
            term_send.at[part],
            term_recv.at[part],
            term_send_sems.at[part],
            term_recv_sems.at[part],
        )

    def part_term(part, which):
        hidden = hidden_buf[pl.ds(part * per_part, per_part)]
        hidden = hidden.reshape(per_part * cap, gate_ref.shape[1])
        term = jnp.dot(hidden, down_ref[which], preferred_element_type=f32)
        return term.astype(bf16).reshape(per_part, cap, half)

    def back_copy(peer):
        return pltpu.make_async_remote_copy(
            src_ref=result_buf.at[peer],
            dst_ref=back_buf.at[me],
            send_sem=back_send_sems.at[peer],
            recv_sem=back_recv_sems.at[me],
            device_id=(peer, core),
            device_id_type=mesh_ids,
        )

    def back_arrival(peer):
        return pltpu.make_async_remote_copy(
            src_ref=result_buf.at[peer],
            dst_ref=back_buf.at[peer],
            send_sem=back_send_sems.at[peer],
            recv_sem=back_recv_sems.at[peer],
            device_id=(peer, core),
            device_id_type=mesh_ids,
        )

    def send_terms(index, carry):
        part = part_at(index)
        term_send[part] = part_term(part, other)
        term_copy(part).start()
        return carry

    lax.fori_loop(0, n_parts, send_terms, 0)

    def own_terms(index, carry):
        part = part_at(index)
        term_own[part] = part_term(part, core)
        return carry

    lax.fori_loop(0, n_parts, own_terms, 0)

    def finish_part(index, carry):
        part = part_at(index)
        term_copy(part).wait_recv()
        total = term_own[part].astype(f32) + term_recv[part].astype(f32)
        result_buf[pl.ds(part * per_part, per_part)] = total.astype(bf16)

        def start_back(inner, carry_inner):
            peer = part * per_part + inner

            @pl.when(peer != me)
            def _():
                back_copy(peer).start()

            return carry_inner

        lax.fori_loop(0, per_part, start_back, 0)
        return carry

    lax.fori_loop(0, n_parts, finish_part, 0)
    back_buf[me] = result_buf[me]

    def finish_sends(step, carry):
        out_copy(step).wait_send()
        back_arrival(peer_at(step)).wait_recv()
        back_copy(peer_at(step)).wait_send()
        return carry

    lax.fori_loop(1, ep_count, finish_sends, 0)

    def finish_pair(step, carry):
        rows_copy(step).wait_send()
        return carry

    lax.fori_loop(0, ep_count, finish_pair, 0)

    def finish_terms(part, carry):
        term_copy(part).wait_send()
        return carry

    lax.fori_loop(0, n_parts, finish_terms, 0)

    back = back_buf[...].reshape(total_rows, half)
    moe_out = jnp.dot(combine_high, back, preferred_element_type=f32)
    moe_out += jnp.dot(combine_low, back, preferred_element_type=f32)
    out_ref[...] = (mid_buf[core].astype(f32) + moe_out).astype(bf16)


def shards(
    tokens_in,
    state_in,
    norm_mix,
    w_recept,
    w_key,
    w_value,
    decay_down,
    decay_up,
    decay_base,
    iclr_down,
    iclr_up,
    iclr_base,
    key_scale,
    key_mix,
    w_out,
    norm_moe,
    router_group,
    router_expert,
    routes,
    expert_gate,
    expert_up,
    expert_down,
):
    f32 = jnp.float32
    bf16 = jnp.bfloat16
    seq_count = tokens_in.shape[0]
    width_model = tokens_in.shape[1]
    heads_here = state_in.shape[1]
    head_size = state_in.shape[-1]
    tp_count = lax.axis_size("tp")
    ep_count = lax.axis_size("ep")

    def split_heads(values):
        return values.astype(f32).reshape(values.shape[0], heads_here, head_size)

    normed = rms_scale(tokens_in, norm_mix)
    recept = jnp.dot(normed, w_recept, preferred_element_type=f32).astype(bf16)
    key_rows = jnp.dot(normed, w_key, preferred_element_type=f32).astype(bf16)
    value_rows = jnp.dot(normed, w_value, preferred_element_type=f32).astype(bf16)
    decay_low = jnp.tanh(jnp.dot(normed, decay_down, preferred_element_type=f32)).astype(bf16)
    iclr_low = jnp.dot(normed, iclr_down, preferred_element_type=f32).astype(bf16)
    log_rate = (
        -jax.nn.softplus(-(decay_base + jnp.dot(decay_low, decay_up, preferred_element_type=f32)))
        - 0.5
    )
    decays = jnp.exp(-jnp.exp(log_rate))
    learn_rate = jax.nn.sigmoid(iclr_base + jnp.dot(iclr_low, iclr_up, preferred_element_type=f32))
    recept_heads = split_heads(recept)
    key_heads = split_heads(key_rows)
    value_heads = split_heads(value_rows)
    rate_heads = split_heads(learn_rate)
    decay_heads = split_heads(decays)
    scaled = key_heads * key_scale.astype(f32).reshape(heads_here, head_size)
    unit_key = scaled * lax.rsqrt(jnp.sum(scaled * scaled, axis=-1, keepdims=True) + 1e-06)
    key_mod = key_heads * (
        1.0 + (rate_heads - 1.0) * key_mix.astype(f32).reshape(heads_here, head_size)
    )
    removed = jnp.einsum("shvk,shk->shv", state_in, unit_key)
    state_out = (
        state_in * decay_heads[:, :, None, :]
        - removed[..., None] * (unit_key * rate_heads)[:, :, None, :]
        + value_heads[..., None] * key_mod[:, :, None, :]
    )
    mixed = (
        jnp.einsum("shvk,shk->shv", state_out, recept_heads)
        .reshape(seq_count, heads_here * head_size)
        .astype(bf16)
    )
    n_groups = router_group.shape[1]
    experts_all = router_expert.shape[1]
    group_size = experts_all // n_groups
    top_count = routes.shape[1]
    half_width = width_model // tp_count
    limit = max(2, 2 * seq_count * top_count // ep_count)
    cap = -(-limit // 16) * 16
    total_rows = experts_all * cap
    group_hit = (routes[:, :1] // group_size == jnp.arange(n_groups)[None, :]).astype(f32)
    uses = jnp.any(routes[:, :, None] == jnp.arange(experts_all)[None, None, :], axis=1)
    position = jnp.cumsum(uses.astype(jnp.int32), axis=0) - 1
    slots = jnp.where(uses, position, -1)
    chooser = (slots[:, :, None] == jnp.arange(cap)[None, None, :]).astype(bf16)
    chooser = chooser.reshape(seq_count, total_rows)
    block_rows = min(total_rows, 256)
    n_parts = min(4, ep_count)
    per_part = ep_count // n_parts
    hidden_width = expert_gate.shape[2]
    down = expert_down[0].reshape(hidden_width, tp_count, half_width).transpose(1, 0, 2)
    dma = pltpu.SemaphoreType.DMA
    layer_out = pl.pallas_call(
        functools.partial(moe_kernel, ep_count, block_rows),
        out_shape=jax.ShapeDtypeStruct((seq_count, half_width), bf16),
        in_specs=[pl.BlockSpec(memory_space=pltpu.VMEM)] * 13,
        out_specs=pl.BlockSpec(memory_space=pltpu.VMEM),
        scratch_shapes=[
            pltpu.VMEM((tp_count, seq_count, half_width), f32),
            pltpu.VMEM((tp_count, seq_count, half_width), f32),
            pltpu.VMEM((tp_count, seq_count, half_width), bf16),
            pltpu.VMEM((tp_count, seq_count, half_width), bf16),
            pltpu.VMEM((ep_count, cap, half_width), bf16),
            pltpu.VMEM((tp_count, ep_count, cap, half_width), bf16),
            pltpu.VMEM((ep_count, cap, hidden_width), bf16),
            pltpu.VMEM((n_parts, per_part, cap, half_width), bf16),
            pltpu.VMEM((n_parts, per_part, cap, half_width), bf16),
            pltpu.VMEM((n_parts, per_part, cap, half_width), bf16),
            pltpu.VMEM((ep_count, cap, half_width), bf16),
            pltpu.VMEM((ep_count, cap, half_width), bf16),
            dma((2,)),
            dma((ep_count,)),
            dma((ep_count,)),
            dma((ep_count,)),
            dma((ep_count,)),
            dma((n_parts,)),
            dma((n_parts,)),
            dma((ep_count,)),
            dma((ep_count,)),
        ],
        compiler_params=pltpu.CompilerParams(
            collective_id=0, has_side_effects=True, vmem_limit_bytes=60 * 1024 * 1024
        ),
    )(
        mixed,
        w_out,
        tokens_in,
        norm_moe.reshape(1, width_model),
        router_group,
        router_expert,
        group_hit,
        uses.astype(f32),
        chooser.T,
        chooser,
        expert_gate[0],
        expert_up[0],
        down,
    )
    return (layer_out, state_out)


def solution(mesh):
    in_specs = (
        P("ep", None),
        P("ep", "tp", None, None),
        P(),
        P(None, "tp"),
        P(None, "tp"),
        P(None, "tp"),
        P(),
        P(None, "tp"),
        P("tp"),
        P(),
        P(None, "tp"),
        P("tp"),
        P("tp"),
        P("tp"),
        P("tp", None),
        P(),
        P(),
        P(),
        P("ep", None),
        P("ep", None, "tp"),
        P("ep", None, "tp"),
        P("ep", "tp", None),
    )
    out_specs = (P("ep", "tp"), P("ep", "tp", None, None))
    return jax.shard_map(shards, mesh=mesh, in_specs=in_specs, out_specs=out_specs, check_vma=False)
```

time: 108 us -> 71.7 us (0.66)
  Pallas kernels: 0 us -> 40.6 us
  blocking collectives: 39.3 us -> 0 us
  waiting for transfers between devices: 21.9 us -> 0 us
  between operations: 14.3 us -> 0.87 us
  starting transfers between devices: 6.81 us -> 0 us
  local copies, waits for them, and re-layouts: 4.48 us -> 9.95 us
  matrix products: 14.8 us -> 10.4 us
  other arithmetic: 6 us -> 9.48 us
    pallas_call x0 -> x1, Pallas kernels: none -> 40.6 us  [shards(): pl.pallas_call(functools.partial(moe_kernel, ep_count, block_rows), out_s...]
    all_to_all x1 -> x0, blocking collectives: 34.7 us -> none  [shards(): lax.all_to_all(outgoing, 'ep', split_axis=0, concat_axis=0, tiled=True)]
    all_to_all x1 -> x0, waiting for transfers between devices: 15.1 us -> none  [shards(): lax.all_to_all(result, 'ep', split_axis=0, concat_axis=0, tiled=True)]
    all_to_all x1 -> x0, starting transfers between devices: 6.77 us -> none  [shards(): lax.all_to_all(result, 'ep', split_axis=0, concat_axis=0, tiled=True)]
    reduce_scatter x1 -> x0, waiting for transfers between devices: 6.75 us -> none  [shards(): lax.psum_scatter(partial_out.astype(jnp.bfloat16), 'tp', scatter_dimensio...]
    psum x1 -> x0, blocking collectives: 4.64 us -> none  [shards(): mixer_out = lax.psum(partial_value, 'tp').astype(bf16)]
    dot_general x8 -> x0, matrix products: 3.76 us -> none  [the longest x1 1.41 us: shards(): partial_out = jnp.dot(hidden, expert_down[0], preferred_element_type=f32)]
    add x1, other arithmetic: 2.75 us -> 5.97 us  [shards(): state_in * decay_heads[:, :, None, :]]
  transfers between devices with their start and end apart: 2 -> 0, of which waited for: 2 -> 0; matrix products, arithmetic and copies ran while one was open for 0% -> 0% of each run, Pallas kernels for 0% -> 0%
where the time goes in v1:
time: 71.7 us; the launch traced here: 71.4 us
  Pallas kernels  40.6 us (57%)
  matrix products  10.4 us (15%)
  local copies, waits for them, and re-layouts  9.95 us (14%)
  other arithmetic  9.48 us (13%)
  between operations  0.87 us (1%)
    pallas_call x1, Pallas kernels, shards(): pl.pallas_call(functools.partial(moe_kernel, ep_count, block_rows), out_s...  40.6 us
    add x1, other arithmetic, shards(): state_in * decay_heads[:, :, None, :]  5.97 us
    unnamed x28, local copies, waits for them, and re-layouts  3.87 us
    dot_general x1, matrix products, shards(): jnp.einsum('shvk,shk->shv', state_out, recept_heads)  3.36 us
    dot_general x1, matrix products, shards(): removed = jnp.einsum('shvk,shk->shv', state_in, unit_key)  3.36 us

profile of v1, /device:TPU:0, one launch (start us, length us, event | category | flops | bytes accessed | tf_op | source)
XLA Modules:
  0.0 71.4 jit_solution(4445621909284264628)
XLA Ops:
  0.7 0.8 %convert_element_type.52 = f32[2048]{0:T(1024)S(1)} convert(bf16[2048]{0:T(1024)(128)(2,1)} %param.24) | non-fusion elementwise | flops 2048 | bytes 12288 | tf_op jit(solution)/shard_map/convert_element_type | solution.py:14
  1.5 1.0 %fusion.8 = f32[32]{0:T(128)S(1)} fusion(bf16[32,2048]{1,0:T(8,128)(2,1)} %tokens_ref.1), kind=kLoop, calls=%fused_computation.18 | loop fusion | flops 196576 | bytes 131200 | tf_op jit(solution)/shard_map/reduce_sum | solution.py:13
  2.6 1.2 %fusion.6 = f32[32,256]{1,0:T(8,128)S(1)} fusion(bf16[2048,256]{1,0:T(8,128)(2,1)S(1)} %copy-done, bf16[32,2048]{1,0:T(8,128)(2,1)} %tokens_ref.1, f32[2048]{0:T(1024)S(1)} %convert_element_type.52, f32[32]{0:T(128)S(1)} %add_rsqrt_fusion.1), kind=kOutput, calls=%fused_computation.12 | convolution fusion | flops 33832960 | bytes 1220736 | tf_op jit(solution)/shard_map/dot_general | solution.py:357
  3.8 0.1 reshape.88
  3.9 0.7 %reshape.89 = f32[4,64]{1,0:T(4,128)S(1)} reshape(bf16[256]{0:T(256)(128)(2,1)} %param.34) | data formatting | bytes 1536 | tf_op jit(solution)/shard_map/mul | solution.py:372
  4.7 0.1 multiply_reduce_fusion
  4.8 1.4 %fusion.3 = f32[32,256]{1,0:T(8,128)S(1)} fusion(bf16[64,256]{1,0:T(8,128)(2,1)} %param.32, bf16[2048,64]{0,1:T(8,128)(2,1)} %param.31, f32[256]{0:T(256)} %param.33, bf16[32,2048]{1,0:T(8,128)(2,1)} %tokens_ref.1, f32[2048]{0:T(1024)S(1)} %convert_element_type.52, f32[32]{0:T(128)S(1)} %add_rsqrt_fusion.1), kind=kOutput, calls=%fused_computation.5 | convolution fusion | flops 9734144 | bytes 468096 | tf_op jit(solution)/shard_map/dot_general | solution.py:366
  6.2 0.1 reshape.84
  6.3 0.7 %reshape.91 = f32[4,64]{1,0:T(4,128)S(1)} reshape(bf16[256]{0:T(256)(128)(2,1)} %param.35) | data formatting | bytes 1536 | tf_op jit(solution)/shard_map/mul | solution.py:375
  7.0 0.1 fusion.26
  7.1 3.4 %fusion.28 = f32[32,4,1,64]{3,2,1,0:T(1,128)S(1)} fusion(f32[32,4,64,1]{2,3,1,0:T(1,128)S(1)} %bitcast.34, f32[32,4,64,64]{3,2,1,0:T(8,128)} %param.23), kind=kOutput, calls=%fused_computation.45 | convolution fusion | flops 1048576 | bytes 2162688 | tf_op jit(solution)/shard_map/shvk,shk->shv/dot_general | solution.py:377
  10.5 0.4 fusion.15
  11.0 0.1 mul.128
  11.1 0.3 fusion.5
  11.4 0.1 reshape.90
  11.5 6.0 %multiply_add_fusion = f32[32,4,64,64]{3,2,1,0:T(8,128)} fusion(f32[32,4,64,64]{3,2,1,0:T(8,128)} %param.23, f32[32,4,64]{2,1,0:T(4,128)S(1)} %get-tuple-element.4, f32[32,4,64]{2,1,0:T(4,128)S(1)} %reshape.90, f32[32,4,64]{2,1,0:T(4,128)S(1)} %get-tuple-element.2, f32[32,4,64]{2,1,0:T(4,128)S(1)} %bitcast.32, f32[32,4,64]{2,1,0:T(4,128)S(1)} %mul.128), kind=kLoop, calls=%fused_computation | loop fusion | flops 2621440 | bytes 4358144 | tf_op jit(solution)/shard_map/add | solution.py:379
  17.5 0.3 convolution_convert_fusion
  17.9 0.1 reshape.97
  18.0 3.4 %fusion.29 = f32[32,4,1,64]{3,2,1,0:T(1,128)S(1)} fusion(f32[32,4,64,64]{3,2,1,0:T(8,128)} %multiply_add_fusion, bf16[32,4,64,1]{2,3,1,0:T(2,128)(2,1)S(1)} %reshape.97), kind=kOutput, calls=%fused_computation.46 | convolution fusion | flops 1048576 | bytes 2146304 | tf_op jit(solution)/shard_map/shvk,shk->shv/dot_general | solution.py:384
  21.4 0.7 convert_element_type.60.mixed_ref
  22.2 0.1 copy.47
  22.6 0.7 %copy.55.placement_ref = bf16[256,32]{1,0:T(8,128)(2,1)} copy(bf16[256,32]{0,1:T(8,128)(2,1)S(1)} %fusion.41) | data formatting | bytes 32768 | tf_op jit(solution)/shard_map/transpose | solution.py:448
  23.3 0.6 compare_convert_fusion.chooser_ref
  23.9 0.7 copy.54.uses_ref
  24.6 0.3 copy.50
  24.9 1.0 %copy.51 = bf16[128,2,1024]{2,0,1:T(8,128)(2,1)} copy(bf16[128,2,1024]{0,2,1:T(8,128)(2,1)S(1)} %bitcast.28) | data formatting | bytes 1048576 | tf_op jit(solution)/shard_map/reshape;squeeze | solution.py:406
  25.9 1.1 %copy.52.router_group_ref = bf16[2048,2]{1,0:T(8,128)(2,1)} copy(bf16[2048,2]{0,1:T(2,128)(2,1)S(1)} %copy-done.6) | data formatting | bytes 16384 | tf_op args[16]
  27.0 1.0 %copy.53.router_expert_ref = bf16[2048,16]{1,0:T(8,128)(2,1)} copy(bf16[2048,16]{0,1:T(8,128)(2,1)S(1)} %copy-done.5) | data formatting | bytes 131072 | tf_op args[17]
  28.0 0.7 fusion.17.group_hit_ref
  28.7 0.6 reshape.86.norm_ref
  29.2 40.6 %shard_map.221 = bf16[32,1024]{1,0:T(8,128)(2,1)} custom-call(bf16[32,256]{1,0:T(8,128)(2,1)} %convert_element_type.60.mixed_ref, bf16[256,2048]{1,0:T(8,128)(2,1)} %w_out_ref.1, bf16[32,2048]{1,0:T(8,128)(2,1)} %tokens_ref.1, bf16[1,2048]{1,0:T(2,128)(2,1)} %reshape.86.norm_ref, bf16[2048,2]{1,0:T(8,128)(2,1)} %copy.52.router_group_ref, ...), custom_call_target="tpu_custom_call" | custom-call | tf_op jit(solution)/shard_map/pallas_call | solution.py:408
  69.9 1.5 %copy.61 = bf16[32,1024]{1,0:T(8,128)(2,1)} copy(bf16[32,1024]{1,0:T(8,128)(2,1)} %shard_map.221) | data formatting | bytes 131072
  (39 shorter events, 0.5 us)
Async XLA Ops:
  0.6 2.0 %copy-start = (bf16[2048,256]{1,0:T(8,128)(2,1)S(1)}, bf16[2048,256]{1,0:T(8,128)(2,1)}, u32[]{:S(2)}) copy-start(bf16[2048,256]{1,0:T(8,128)(2,1)} %param.26) | copy-start | bytes 3145732
  0.6 9.9 %copy-start.1 = (bf16[32,2048]{1,0:T(8,128)(2,1)S(1)}, bf16[32,2048]{1,0:T(8,128)(2,1)}, u32[]{:S(2)}) copy-start(bf16[32,2048]{1,0:T(8,128)(2,1)} %tokens_ref.1) | copy-start | bytes 393220
  0.7 9.8 %copy-start.9 = (bf16[2048,64]{0,1:T(8,128)(2,1)S(1)}, bf16[2048,64]{0,1:T(8,128)(2,1)}, u32[]{:S(2)}) copy-start(bf16[2048,64]{0,1:T(8,128)(2,1)} %param.28) | copy-start | bytes 786436
  0.7 9.8 %copy-start.10 = (bf16[64,256]{1,0:T(8,128)(2,1)S(1)}, bf16[64,256]{1,0:T(8,128)(2,1)}, u32[]{:S(2)}) copy-start(bf16[64,256]{1,0:T(8,128)(2,1)} %param.29) | copy-start | bytes 98308
  0.7 9.8 %copy-start.11 = (f32[256]{0:T(256)S(1)}, f32[256]{0:T(256)}, u32[]{:S(2)}) copy-start(f32[256]{0:T(256)} %param.30) | copy-start | bytes 3076
  0.7 10.4 %copy-start.2 = (bf16[2048,256]{1,0:T(8,128)(2,1)S(1)}, bf16[2048,256]{1,0:T(8,128)(2,1)}, u32[]{:S(2)}) copy-start(bf16[2048,256]{1,0:T(8,128)(2,1)} %param.27) | copy-start | bytes 3145732
  11.5 6.0 %copy-start.3 = (bf16[2048,256]{1,0:T(8,128)(2,1)S(1)}, bf16[2048,256]{1,0:T(8,128)(2,1)}, u32[]{:S(2)}) copy-start(bf16[2048,256]{1,0:T(8,128)(2,1)} %param.25) | copy-start | bytes 3145732
  17.5 4.6 %copy-start.8 = (s32[32,4]{0,1:T(4,128)S(1)}, s32[32,4]{0,1:T(4,128)}, u32[]{:S(2)}) copy-start(s32[32,4]{0,1:T(4,128)} %param.40) | copy-start | bytes 1540
  17.5 7.1 %copy-start.4 = (bf16[1,128,2048]{2,1,0:T(8,128)(2,1)S(1)}, bf16[1,128,2048]{2,1,0:T(8,128)(2,1)}, u32[]{:S(2)}) copy-start(bf16[1,128,2048]{2,1,0:T(8,128)(2,1)} %param.43) | copy-start | bytes 1572868
  17.5 8.4 %copy-start.6 = (bf16[2048,2]{0,1:T(2,128)(2,1)S(1)}, bf16[2048,2]{0,1:T(2,128)(2,1)}, u32[]{:S(2)}) copy-start(bf16[2048,2]{0,1:T(2,128)(2,1)} %param.38) | copy-start | bytes 24580
  17.8 9.1 %copy-start.5 = (bf16[2048,16]{0,1:T(8,128)(2,1)S(1)}, bf16[2048,16]{0,1:T(8,128)(2,1)}, u32[]{:S(2)}) copy-start(bf16[2048,16]{0,1:T(8,128)(2,1)} %param.39) | copy-start | bytes 196612
  18.0 10.7 %copy-start.7 = (bf16[2048]{0:T(1024)(128)(2,1)S(1)}, bf16[2048]{0:T(1024)(128)(2,1)}, u32[]{:S(2)}) copy-start(bf16[2048]{0:T(1024)(128)(2,1)} %param.37) | copy-start | bytes 12292

commit v2 on v1

--- a/solution.py
+++ b/solution.py
@@ -8,29 +8,144 @@
 from jax.sharding import PartitionSpec as P
 
 
-def rms_scale(values, weights):
-    values32 = values.astype(jnp.float32)
-    factor = lax.rsqrt(jnp.mean(values32 * values32, axis=-1, keepdims=True) + 1e-06)
-    return (values32 * factor * weights.astype(jnp.float32)).astype(jnp.bfloat16)
+def mixer_kernel(
+    tokens_ref,
+    norm_ref,
+    w_recept_hbm,
+    w_key_hbm,
+    w_value_hbm,
+    decay_down_ref,
+    decay_up_ref,
+    decay_base_ref,
+    iclr_down_ref,
+    iclr_up_ref,
+    iclr_base_ref,
+    key_scale_ref,
+    key_mix_ref,
+    state_hbm,
+    mixed_ref,
+    state_out_hbm,
+    weights,
+    state_buf,
+    out_buf,
+    vectors,
+    value_t,
+    mixed_t,
+    weight_sems,
+    in_sems,
+    out_sems,
+):
+    f32 = jnp.float32
+    bf16 = jnp.bfloat16
+    seq_count, width = tokens_ref.shape
+    heads, head_size = state_hbm.shape[1], state_hbm.shape[3]
+    channels = heads * head_size
+    n_chunks = in_sems.shape[0]
+    per_chunk = seq_count // n_chunks
+    rows_dims = (((1,), (1,)), ((), ()))
+    weight_loads = [
+        pltpu.make_async_copy(source, weights.at[index], weight_sems.at[index])
+        for index, source in enumerate((w_key_hbm, w_value_hbm, w_recept_hbm))
+    ]
+    for load in weight_loads:
+        load.start()
+    state_loads = []
+    state_stores = []
+    for index in range(n_chunks):
+        span = pl.ds(index * per_chunk, per_chunk)
+        state_loads.append(
+            pltpu.make_async_copy(state_hbm.at[span], state_buf.at[span], in_sems.at[index])
+        )
+        state_stores.append(
+            pltpu.make_async_copy(out_buf.at[span], state_out_hbm.at[span], out_sems.at[index])
+        )
+        state_loads[index].start()
+
+    tokens = tokens_ref[...].astype(f32)
+    factor = lax.rsqrt(jnp.mean(tokens * tokens, axis=1, keepdims=True) + 1e-06)
+    normed = (tokens * factor * norm_ref[...].reshape(1, width).astype(f32)).astype(bf16)
+    decay_low = jnp.tanh(
+        lax.dot_general(normed, decay_down_ref[...], rows_dims, preferred_element_type=f32)
+    ).astype(bf16)
+    iclr_low = lax.dot_general(
+        normed, iclr_down_ref[...], rows_dims, preferred_element_type=f32
+    ).astype(bf16)
+    decay_in = decay_base_ref[...].reshape(1, channels) + jnp.dot(
+        decay_low, decay_up_ref[...], preferred_element_type=f32
+    )
+    decays = jnp.exp(-jnp.exp(jnp.float32(-0.5)) * jax.nn.sigmoid(decay_in))
+    rate = jax.nn.sigmoid(
+        iclr_base_ref[...].reshape(1, channels)
+        + jnp.dot(iclr_low, iclr_up_ref[...], preferred_element_type=f32)
+    )
+    projected = []
+    for index in range(3):
+        weight_loads[index].wait()
+        rows = jnp.dot(normed, weights[index], preferred_element_type=f32)
+        projected.append(rows.astype(bf16).astype(f32))
+    key, value, recept = projected
+    value_t[...] = value.T
+    scaled = key * key_scale_ref[...].reshape(1, channels).astype(f32)
+    key_mod = key * (1.0 + (rate - 1.0) * key_mix_ref[...].reshape(1, channels).astype(f32))
+    for head in range(heads):
+        span = slice(head * head_size, (head + 1) * head_size)
+        part = scaled[:, span]
+        unit = part * lax.rsqrt(jnp.sum(part * part, axis=1, keepdims=True) + 1e-06)
+        vectors[0, head] = decays[:, span]
+        vectors[1, head] = unit
+        vectors[2, head] = unit * rate[:, span]
+        vectors[3, head] = key_mod[:, span]
+        vectors[4, head] = recept[:, span]
+
+    lanes = lax.broadcasted_iota(jnp.int32, (head_size, seq_count), 1)
+
+    def update(seq, carry):
+        here = lanes == seq
+        for head in range(heads):
+            span = slice(head * head_size, (head + 1) * head_size)
+            row = pl.ds(seq, 1)
+            state = state_buf[seq, head]
+            removed = jnp.sum(state * vectors[1, head, row, :], axis=1, keepdims=True)
+            column = jnp.sum(jnp.where(here, value_t[span, :], 0.0), axis=1, keepdims=True)
+            state = (
+                state * vectors[0, head, row, :]
+                - removed * vectors[2, head, row, :]
+                + column * vectors[3, head, row, :]
+            )
+            out_buf[seq, head] = state
+            mixed = jnp.sum(state * vectors[4, head, row, :], axis=1, keepdims=True)
+            mixed_t[span, :] = jnp.where(here, mixed, mixed_t[span, :])
+        return carry
+
+    mixed_t[...] = jnp.zeros_like(mixed_t)
+    for index in range(n_chunks):
+        state_loads[index].wait()
+        lax.fori_loop(index * per_chunk, (index + 1) * per_chunk, update, 0, unroll=2)
+        state_stores[index].start()
+    mixed_ref[...] = mixed_t[...].T.astype(bf16)
+    for store in state_stores:
+        store.wait()
 
 
 def moe_kernel(
     ep_count,
     block_rows,
     mixed_ref,
-    w_out_ref,
+    w_out_hbm,
     tokens_ref,
     norm_ref,
     router_group_ref,
     router_expert_ref,
-    group_hit_ref,
-    uses_ref,
-    placement_ref,
-    chooser_ref,
+    routes_ref,
+    gate_hbm,
+    up_hbm,
+    down_hbm,
+    moe_ref,
+    mid_ref,
     gate_ref,
     up_ref,
     down_ref,
-    out_ref,
+    w_out_ref,
     part_buf,
     part_recv,
     mid_buf,
@@ -52,6 +167,7 @@
     term_recv_sems,
     back_send_sems,
     back_recv_sems,
+    load_sems,
 ):
     f32 = jnp.float32
     bf16 = jnp.bfloat16
@@ -83,6 +199,39 @@
 
     lax.fori_loop(1, ep_count, greet, 0)
 
+    loads = [
+        pltpu.make_async_copy(w_out_hbm, w_out_ref, load_sems.at[0]),
+        pltpu.make_async_copy(gate_hbm.at[0], gate_ref, load_sems.at[1]),
+        pltpu.make_async_copy(up_hbm.at[0], up_ref, load_sems.at[2]),
+        pltpu.make_async_copy(down_hbm.at[0, :, pl.ds(0, half)], down_ref.at[0], load_sems.at[3]),
+        pltpu.make_async_copy(down_hbm.at[0, :, pl.ds(half, half)], down_ref.at[1], load_sems.at[4]),
+    ]
+    for load in loads:
+        load.start()
+
+    n_groups = router_group_ref.shape[0]
+    expert_ids = lax.broadcasted_iota(jnp.int32, (ep_count, seq_count), 0)
+    uses = jnp.zeros((ep_count, seq_count), f32)
+    for index in range(routes_ref.shape[0]):
+        uses += jnp.where(routes_ref[index : index + 1, :] == expert_ids, 1.0, 0.0)
+    group_ids = lax.broadcasted_iota(jnp.int32, (n_groups, seq_count), 0)
+    group_hit = jnp.where(
+        routes_ref[0:1, :] // (ep_count // n_groups) == group_ids, 1.0, 0.0
+    )
+    row_ids = lax.broadcasted_iota(jnp.int32, (seq_count, seq_count), 0)
+    column_ids = lax.broadcasted_iota(jnp.int32, (seq_count, seq_count), 1)
+    earlier = jnp.where(row_ids < column_ids, 1.0, 0.0).astype(bf16)
+    position = jnp.dot(uses.astype(bf16), earlier, preferred_element_type=f32)
+    slots = jnp.where(uses > 0.5, position, -1.0).astype(bf16)
+    slot_rows = lax.broadcasted_iota(jnp.int32, (total_rows, ep_count), 0)
+    slot_experts = lax.broadcasted_iota(jnp.int32, (total_rows, ep_count), 1)
+    spread = jnp.where(slot_rows // cap == slot_experts, 1.0, 0.0).astype(bf16)
+    slot_of_row = lax.broadcasted_iota(jnp.int32, (total_rows, seq_count), 0) % cap
+    hits = jnp.dot(spread, slots, preferred_element_type=f32) == slot_of_row.astype(f32)
+    chooser = jnp.where(hits, 1.0, 0.0)
+    placement = chooser.astype(bf16)
+
+    loads[0].wait()
     for index in range(2):
         columns = slice(index * half, (index + 1) * half)
         part_buf[index] = jnp.dot(
@@ -116,13 +265,13 @@
     for index in range(2):
         columns = slice(index * half, (index + 1) * half)
         norm_buf[index] = (
-            mid_buf[index].astype(f32) * factor * norm_ref[:, columns].astype(f32)
+            mid_buf[index].astype(f32) * factor * norm_ref[columns].reshape(1, half).astype(f32)
         ).astype(bf16)
 
     own_norm = norm_buf[core]
     for index in range(n_blocks):
         rows = jnp.dot(
-            placement_ref[index * block_rows : (index + 1) * block_rows, :],
+            placement[index * block_rows : (index + 1) * block_rows, :],
             own_norm,
             preferred_element_type=f32,
         ).astype(bf16)
@@ -165,27 +314,27 @@
     rows_buf[core, me] = send_buf[me]
     rows_copy(0).start()
 
-    group_logit = jnp.zeros(group_hit_ref.shape, f32)
-    expert_logit = jnp.zeros(uses_ref.shape, f32)
+    rows_dims = (((1,), (1,)), ((), ()))
+    group_logit = jnp.zeros(group_hit.shape, f32)
+    expert_logit = jnp.zeros(uses.shape, f32)
     for index in range(2):
         columns = slice(index * half, (index + 1) * half)
-        group_logit += jnp.dot(
-            norm_buf[index], router_group_ref[columns, :], preferred_element_type=f32
-        )
-        expert_logit += jnp.dot(
-            norm_buf[index], router_expert_ref[columns, :], preferred_element_type=f32
-        )
-    group_prob = jax.nn.sigmoid(jnp.sum(group_logit * group_hit_ref[...], axis=1, keepdims=True))
-    scores = jax.nn.sigmoid(expert_logit) * uses_ref[...]
-    weights = group_prob * scores / jnp.sum(scores, axis=1, keepdims=True)
+        group_logit += lax.dot_general(
+            router_group_ref[:, columns], norm_buf[index], rows_dims, preferred_element_type=f32
+        )
+        expert_logit += lax.dot_general(
+            router_expert_ref[:, columns], norm_buf[index], rows_dims, preferred_element_type=f32
+        )
+    group_prob = jax.nn.sigmoid(jnp.sum(group_logit * group_hit, axis=0, keepdims=True))
+    scores = jax.nn.sigmoid(expert_logit) * uses
+    weights = group_prob * scores / jnp.sum(scores, axis=0, keepdims=True)
     weights_high = weights.astype(bf16)
     weights_low = (weights - weights_high.astype(f32)).astype(bf16)
-    slot_expert = lax.broadcasted_iota(jnp.int32, (ep_count, total_rows), 1) // cap
-    expert_ids = lax.broadcasted_iota(jnp.int32, (ep_count, total_rows), 0)
-    spread = jnp.where(slot_expert == expert_ids, 1.0, 0.0).astype(bf16)
-    chooser = chooser_ref[...].astype(f32)
-    combine_high = (jnp.dot(weights_high, spread, preferred_element_type=f32) * chooser).astype(bf16)
-    combine_low = (jnp.dot(weights_low, spread, preferred_element_type=f32) * chooser).astype(bf16)
+    combine_high = (jnp.dot(spread, weights_high, preferred_element_type=f32) * chooser).T
+    combine_low = (jnp.dot(spread, weights_low, preferred_element_type=f32) * chooser).T
+    combine_high = combine_high.astype(bf16)
+    combine_low = combine_low.astype(bf16)
+    mid_ref[...] = mid_buf[core]
 
     def relay(index, carry):
         step = step_at(ep_count - 2 - index)
@@ -201,6 +350,8 @@
 
     lax.fori_loop(0, ep_count, arrive, 0)
 
+    for load in loads[1:]:
+        load.wait()
     for index in range(n_blocks):
         experts = slice(index * per_block, (index + 1) * per_block)
         gate_part = jnp.zeros((block_rows, gate_ref.shape[1]), f32)
@@ -313,7 +464,7 @@
     back = back_buf[...].reshape(total_rows, half)
     moe_out = jnp.dot(combine_high, back, preferred_element_type=f32)
     moe_out += jnp.dot(combine_low, back, preferred_element_type=f32)
-    out_ref[...] = (mid_buf[core].astype(f32) + moe_out).astype(bf16)
+    moe_ref[...] = moe_out
 
 
 def shards(
@@ -342,75 +493,72 @@
 ):
     f32 = jnp.float32
     bf16 = jnp.bfloat16
-    seq_count = tokens_in.shape[0]
-    width_model = tokens_in.shape[1]
-    heads_here = state_in.shape[1]
-    head_size = state_in.shape[-1]
+    seq_count, width_model = tokens_in.shape
+    heads_here, head_size = state_in.shape[1], state_in.shape[3]
+    channels = heads_here * head_size
     tp_count = lax.axis_size("tp")
     ep_count = lax.axis_size("ep")
-
-    def split_heads(values):
-        return values.astype(f32).reshape(values.shape[0], heads_here, head_size)
-
-    normed = rms_scale(tokens_in, norm_mix)
-    recept = jnp.dot(normed, w_recept, preferred_element_type=f32).astype(bf16)
-    key_rows = jnp.dot(normed, w_key, preferred_element_type=f32).astype(bf16)
-    value_rows = jnp.dot(normed, w_value, preferred_element_type=f32).astype(bf16)
-    decay_low = jnp.tanh(jnp.dot(normed, decay_down, preferred_element_type=f32)).astype(bf16)
-    iclr_low = jnp.dot(normed, iclr_down, preferred_element_type=f32).astype(bf16)
-    log_rate = (
-        -jax.nn.softplus(-(decay_base + jnp.dot(decay_low, decay_up, preferred_element_type=f32)))
-        - 0.5
+    dma = pltpu.SemaphoreType.DMA
+    vmem = pl.BlockSpec(memory_space=pltpu.VMEM)
+    anywhere = pl.BlockSpec(memory_space=pl.ANY)
+    n_chunks = 4 if seq_count % 4 == 0 else 1
+    mixed, state_out = pl.pallas_call(
+        mixer_kernel,
+        out_shape=(
+            jax.ShapeDtypeStruct((seq_count, channels), bf16),
+            jax.ShapeDtypeStruct(state_in.shape, f32),
+        ),
+        in_specs=[vmem] * 2 + [anywhere] * 3 + [vmem] * 8 + [anywhere],
+        out_specs=(vmem, anywhere),
+        scratch_shapes=[
+            pltpu.VMEM((3, width_model, channels), bf16),
+            pltpu.VMEM(state_in.shape, f32),
+            pltpu.VMEM(state_in.shape, f32),
+            pltpu.VMEM((5, heads_here, seq_count, head_size), f32),
+            pltpu.VMEM((channels, seq_count), f32),
+            pltpu.VMEM((channels, seq_count), f32),
+            dma((3,)),
+            dma((n_chunks,)),
+            dma((n_chunks,)),
+        ],
+        compiler_params=pltpu.CompilerParams(vmem_limit_bytes=60 * 1024 * 1024),
+    )(
+        tokens_in,
+        norm_mix,
+        w_recept,
+        w_key,
+        w_value,
+        decay_down.T,
+        decay_up,
+        decay_base,
+        iclr_down.T,
+        iclr_up,
+        iclr_base,
+        key_scale,
+        key_mix,
+        state_in,
     )
-    decays = jnp.exp(-jnp.exp(log_rate))
-    learn_rate = jax.nn.sigmoid(iclr_base + jnp.dot(iclr_low, iclr_up, preferred_element_type=f32))
-    recept_heads = split_heads(recept)
-    key_heads = split_heads(key_rows)
-    value_heads = split_heads(value_rows)
-    rate_heads = split_heads(learn_rate)
-    decay_heads = split_heads(decays)
-    scaled = key_heads * key_scale.astype(f32).reshape(heads_here, head_size)
-    unit_key = scaled * lax.rsqrt(jnp.sum(scaled * scaled, axis=-1, keepdims=True) + 1e-06)
-    key_mod = key_heads * (
-        1.0 + (rate_heads - 1.0) * key_mix.astype(f32).reshape(heads_here, head_size)
-    )
-    removed = jnp.einsum("shvk,shk->shv", state_in, unit_key)
-    state_out = (
-        state_in * decay_heads[:, :, None, :]
-        - removed[..., None] * (unit_key * rate_heads)[:, :, None, :]
-        + value_heads[..., None] * key_mod[:, :, None, :]
-    )
-    mixed = (
-        jnp.einsum("shvk,shk->shv", state_out, recept_heads)
-        .reshape(seq_count, heads_here * head_size)
-        .astype(bf16)
-    )
-    n_groups = router_group.shape[1]
-    experts_all = router_expert.shape[1]
-    group_size = experts_all // n_groups
     top_count = routes.shape[1]
     half_width = width_model // tp_count
     limit = max(2, 2 * seq_count * top_count // ep_count)
     cap = -(-limit // 16) * 16
-    total_rows = experts_all * cap
-    group_hit = (routes[:, :1] // group_size == jnp.arange(n_groups)[None, :]).astype(f32)
-    uses = jnp.any(routes[:, :, None] == jnp.arange(experts_all)[None, None, :], axis=1)
-    position = jnp.cumsum(uses.astype(jnp.int32), axis=0) - 1
-    slots = jnp.where(uses, position, -1)
-    chooser = (slots[:, :, None] == jnp.arange(cap)[None, None, :]).astype(bf16)
-    chooser = chooser.reshape(seq_count, total_rows)
-    block_rows = min(total_rows, 256)
+    block_rows = min(ep_count * cap, 256)
     n_parts = min(4, ep_count)
     per_part = ep_count // n_parts
     hidden_width = expert_gate.shape[2]
-    down = expert_down[0].reshape(hidden_width, tp_count, half_width).transpose(1, 0, 2)
-    dma = pltpu.SemaphoreType.DMA
-    layer_out = pl.pallas_call(
+    moe_out, mid_half = pl.pallas_call(
         functools.partial(moe_kernel, ep_count, block_rows),
-        out_shape=jax.ShapeDtypeStruct((seq_count, half_width), bf16),
-        in_specs=[pl.BlockSpec(memory_space=pltpu.VMEM)] * 13,
-        out_specs=pl.BlockSpec(memory_space=pltpu.VMEM),
+        out_shape=(
+            jax.ShapeDtypeStruct((seq_count, half_width), f32),
+            jax.ShapeDtypeStruct((seq_count, half_width), bf16),
+        ),
+        in_specs=[vmem, anywhere] + [vmem] * 5 + [anywhere] * 3,
+        out_specs=(vmem, vmem),
         scratch_shapes=[
+            pltpu.VMEM((width_model, hidden_width), bf16),
+            pltpu.VMEM((width_model, hidden_width), bf16),
+            pltpu.VMEM((tp_count, hidden_width, half_width), bf16),
+            pltpu.VMEM(w_out.shape, bf16),
             pltpu.VMEM((tp_count, seq_count, half_width), f32),
             pltpu.VMEM((tp_count, seq_count, half_width), f32),
             pltpu.VMEM((tp_count, seq_count, half_width), bf16),
@@ -432,6 +580,7 @@
             dma((n_parts,)),
             dma((ep_count,)),
             dma((ep_count,)),
+            dma((5,)),
         ],
         compiler_params=pltpu.CompilerParams(
             collective_id=0, has_side_effects=True, vmem_limit_bytes=60 * 1024 * 1024
@@ -440,17 +589,15 @@
         mixed,
         w_out,
         tokens_in,
-        norm_moe.reshape(1, width_model),
-        router_group,
-        router_expert,
-        group_hit,
-        uses.astype(f32),
-        chooser.T,
-        chooser,
-        expert_gate[0],
-        expert_up[0],
-        down,
+        norm_moe,
+        router_group.T,
+        router_expert.T,
+        routes.T,
+        expert_gate,
+        expert_up,
+        expert_down,
     )
+    layer_out = (mid_half.astype(f32) + moe_out).astype(bf16)
     return (layer_out, state_out)
 
 

time: 71.7 us -> 56.2 us (0.78)
  Pallas kernels: 40.6 us -> 53.8 us
  matrix products: 10.4 us -> 0 us
  local copies, waits for them, and re-layouts: 9.95 us -> 0 us
  other arithmetic: 9.48 us -> 1.55 us
    pallas_call x0 -> x1, Pallas kernels: none -> 14.2 us  [shards(): pl.pallas_call(mixer_kernel, out_shape=(jax.ShapeDtypeStruct((seq_count,...]
    dot_general x7 -> x0, matrix products: 10.4 us -> none  [the longest x1 3.36 us: shards(): jnp.einsum('shvk,shk->shv', state_out, recept_heads)]
    add x1 -> x0, other arithmetic: 5.97 us -> none  [shards(): state_in * decay_heads[:, :, None, :]]
    unnamed x28 -> x0, local copies, waits for them, and re-layouts: 3.87 us -> none
    mul x4 -> x0, local copies, waits for them, and re-layouts: 1.67 us -> none  [the longest x1 0.74 us: shards(): scaled = key_heads * key_scale.astype(f32).reshape(heads_here, head_size)]
    convert_element_type x3 -> x0, local copies, waits for them, and re-layouts: 1.45 us -> none  [the longest x1 0.7 us: shards(): mixed = jnp.einsum('shvk,shk->shv', state_out, recept_heads).reshape(seq_...]
    reduce_sum x2 -> x0, other arithmetic: 1.14 us -> none  [the longest x1 1.04 us: rms_scale(): jnp.mean(values32 * values32, axis=-1, keepdims=True) + 1e-06]
    pallas_call x1, Pallas kernels: 40.6 us -> 39.5 us  [shards(): pl.pallas_call(functools.partial(moe_kernel, ep_count, block_rows), out_s...]
where the time goes in v2:
time: 56.2 us; the launch traced here: 56 us
  Pallas kernels  53.8 us (96%)
  other arithmetic  1.55 us (3%)
  between operations  0.65 us (1%)
    pallas_call x1, Pallas kernels, shards(): pl.pallas_call(functools.partial(moe_kernel, ep_count, block_rows), out_s...  39.5 us
    pallas_call x1, Pallas kernels, shards(): pl.pallas_call(mixer_kernel, out_shape=(jax.ShapeDtypeStruct((seq_count,...  14.2 us
    convert_element_type x1, other arithmetic, shards(): layer_out = (mid_half.astype(f32) + moe_out).astype(bf16)  1.55 us

profile of v2, /device:TPU:0, one launch (start us, length us, event | category | flops | bytes accessed | tf_op | source)
XLA Modules:
  0.0 56.0 jit_solution(8745259136601089880)
XLA Ops:
  0.6 14.2 %shard_map.221 = (bf16[32,256]{1,0:T(8,128)(2,1)}, f32[32,4,64,64]{3,2,1,0:T(8,128)}) custom-call(bf16[32,2048]{1,0:T(8,128)(2,1)} %tokens_ref.3, bf16[2048]{0:T(1024)(128)(2,1)} %norm_ref.2, bf16[2048,256]{1,0:T(8,128)(2,1)} %w_recept_hbm.1, bf16[2048,256]{1,0:T(8,128)(2,1)} %w_key_hbm.1, bf16[2048,256]{1,0:T(8,128)(2,1)} %w_value_hbm.1, ...), custom_call_target="tpu_custom_call" | custom-call | tf_op jit(solution)/shard_map/pallas_call | solution.py:505
  14.9 39.5 %shard_map.222 = (f32[32,1024]{1,0:T(8,128)}, bf16[32,1024]{1,0:T(8,128)(2,1)}) custom-call(bf16[32,256]{1,0:T(8,128)(2,1)} %get-tuple-element.6.mixed_ref, bf16[256,2048]{1,0:T(8,128)(2,1)} %w_out_hbm.1, bf16[32,2048]{1,0:T(8,128)(2,1)} %tokens_ref.3, bf16[2048]{0:T(1024)(128)(2,1)} %norm_ref.3, bf16[2,2048]{1,0:T(2,128)(2,1)} %bitcast.8, ...), custom_call_target="tpu_custom_call" | custom-call | tf_op jit(solution)/shard_map/pallas_call | solution.py:549
  54.4 1.6 %add_convert_fusion = bf16[32,1024]{1,0:T(8,128)(2,1)} fusion(f32[32,1024]{1,0:T(8,128)} %get-tuple-element.8, bf16[32,1024]{1,0:T(8,128)(2,1)} %get-tuple-element.7), kind=kLoop, calls=%fused_computation | loop fusion | flops 98304 | bytes 262144 | tf_op jit(solution)/shard_map/convert_element_type | solution.py:600

commit v3 on v2

--- a/solution.py
+++ b/solution.py
@@ -120,7 +120,7 @@
     mixed_t[...] = jnp.zeros_like(mixed_t)
     for index in range(n_chunks):
         state_loads[index].wait()
-        lax.fori_loop(index * per_chunk, (index + 1) * per_chunk, update, 0, unroll=2)
+        lax.fori_loop(index * per_chunk, (index + 1) * per_chunk, update, 0, unroll=4)
         state_stores[index].start()
     mixed_ref[...] = mixed_t[...].T.astype(bf16)
     for store in state_stores:
@@ -337,7 +337,7 @@
     mid_ref[...] = mid_buf[core]
 
     def relay(index, carry):
-        step = step_at(ep_count - 2 - index)
+        step = step_at(index)
         out_copy(step).wait_recv()
         rows_copy(step).start()
         return carry

time: 56.2 us -> 57.5 us (1.023)
  Pallas kernels: 53.8 us -> 55.1 us
    pallas_call x1, Pallas kernels: 14.2 us -> 16.2 us  [shards(): pl.pallas_call(mixer_kernel, out_shape=(jax.ShapeDtypeStruct((seq_count,...]
    pallas_call x1, Pallas kernels: 39.5 us -> 38.9 us  [shards(): pl.pallas_call(functools.partial(moe_kernel, ep_count, block_rows), out_s...]
where the time goes in v3:
time: 57.5 us; the launch traced here: 57.3 us
  Pallas kernels  55.1 us (96%)
  other arithmetic  1.55 us (3%)
  between operations  0.65 us (1%)
    pallas_call x1, Pallas kernels, shards(): pl.pallas_call(functools.partial(moe_kernel, ep_count, block_rows), out_s...  38.9 us
    pallas_call x1, Pallas kernels, shards(): pl.pallas_call(mixer_kernel, out_shape=(jax.ShapeDtypeStruct((seq_count,...  16.2 us
    convert_element_type x1, other arithmetic, shards(): layer_out = (mid_half.astype(f32) + moe_out).astype(bf16)  1.55 us

profile of v3, /device:TPU:0, one launch (start us, length us, event | category | flops | bytes accessed | tf_op | source)
XLA Modules:
  0.0 57.3 jit_solution(7473378468319673668)
XLA Ops:
  0.6 16.2 %shard_map.221 = (bf16[32,256]{1,0:T(8,128)(2,1)}, f32[32,4,64,64]{3,2,1,0:T(8,128)}) custom-call(bf16[32,2048]{1,0:T(8,128)(2,1)} %tokens_ref.3, bf16[2048]{0:T(1024)(128)(2,1)} %norm_ref.2, bf16[2048,256]{1,0:T(8,128)(2,1)} %w_recept_hbm.1, bf16[2048,256]{1,0:T(8,128)(2,1)} %w_key_hbm.1, bf16[2048,256]{1,0:T(8,128)(2,1)} %w_value_hbm.1, ...), custom_call_target="tpu_custom_call" | custom-call | tf_op jit(solution)/shard_map/pallas_call | solution.py:505
  16.9 38.9 %shard_map.222 = (f32[32,1024]{1,0:T(8,128)}, bf16[32,1024]{1,0:T(8,128)(2,1)}) custom-call(bf16[32,256]{1,0:T(8,128)(2,1)} %get-tuple-element.6.mixed_ref, bf16[256,2048]{1,0:T(8,128)(2,1)} %w_out_hbm.1, bf16[32,2048]{1,0:T(8,128)(2,1)} %tokens_ref.3, bf16[2048]{0:T(1024)(128)(2,1)} %norm_ref.3, bf16[2,2048]{1,0:T(2,128)(2,1)} %bitcast.8, ...), custom_call_target="tpu_custom_call" | custom-call | tf_op jit(solution)/shard_map/pallas_call | solution.py:549
  55.8 1.6 %add_convert_fusion = bf16[32,1024]{1,0:T(8,128)(2,1)} fusion(f32[32,1024]{1,0:T(8,128)} %get-tuple-element.8, bf16[32,1024]{1,0:T(8,128)(2,1)} %get-tuple-element.7), kind=kLoop, calls=%fused_computation | loop fusion | flops 98304 | bytes 262144 | tf_op jit(solution)/shard_map/convert_element_type | solution.py:600
